TPU v7x, 256 devices: a whole 4x4x8 slice. The times are simulated.
256 devices in a mesh: ep: 64 (over z, x, core), tp: 4 (over y).
Axes of the slice: x: 4, y: 4, z: 8, core: 2. Of those that a mesh axis runs over, the one named last changes fastest.
Arguments:
- queries: bfloat16 [16384, 1024], P('ep', 'tp'), may hold values from -192 to 192
- keys_values: bfloat16 [16384, 512], P('ep', 'tp'), may hold values from -192 to 192
- log_gate_cum: float32 [16, 16384], P('tp'), as said below
- mix_weight: bfloat16 [1024, 2048], P('tp'), may hold values from -0.1875 to 0.1875
- mix_gain: float32 [2048], replicated, may hold values from 0.1 to 1.9
- moe_in: bfloat16 [49152, 2048], P(('ep', 'tp')), may hold values from -6 to 6
- moe_gain: float32 [2048], replicated, may hold values from 0.1 to 1.9
- routes: int32 [49152, 2], P(('ep', 'tp')), may hold values from 0 to 63, all different within a row; in each aligned block of 192 rows (0 to 191, 192 to 383, ...) at most 9 rows name the same one
- route_weight: float32 [49152, 2], P(('ep', 'tp')), may hold values from 0.25 to 2
- expert_gate: bfloat16 [64, 2048, 1024], P('ep', None, 'tp'), may hold values from -0.125 to 0.125
- expert_up: bfloat16 [64, 2048, 1024], P('ep', None, 'tp'), may hold values from -0.125 to 0.125
- expert_down: bfloat16 [64, 1024, 2048], P('ep', 'tp'), may hold values from -0.1875 to 0.1875
Outputs:
- mix_result: bfloat16 [16384, 2048], P(('ep', 'tp'))
- moe_result: bfloat16 [49152, 2048], P(('ep', 'tp'))
Inputs may be any that keep to these rules, and one draw needn't show every extreme that they name: `log_gate_cum`: along positions each head's values never rise. `routes`: each row names 2 different experts. Among the rows of one device no expert is named more than 9 times, and in every draw some device names some expert exactly 9 times.
All inputs are finite; a program needn't handle non-finite values.
Results may differ from a plain program's by a relative error of at most 0.013.
Values may be sent and summed in bfloat16 or wider, within the bound.
A program may use at most 128 MiB of HBM per device.

v0:
```python
from functools import partial
import math

import jax
import jax.numpy as jnp
from jax import lax
from jax.sharding import PartitionSpec as P

HEAD = 64


EPSILON = 1e-06
NEGATIVE = -1e30


def sent_together(arrays, axis, dim, along):
    ends, at = ([], 0)
    for a in arrays[:-1]:
        at += a.shape[along]
        ends.append(at)
    both = jnp.concatenate(arrays, axis=along)
    return tuple(jnp.split(lax.all_gather(both, axis, axis=dim, tiled=True), ends, axis=along))


def cut_along(shard, dim, count):
    before, after = (shard.shape[:dim], shard.shape[dim + 1 :])
    return jnp.moveaxis(shard.reshape(*before, count, -1, *after), dim, 0)


def sum_at_owner(shard, axis, dim):
    count = lax.axis_size(axis)
    blocks = lax.all_to_all(cut_along(shard, dim, count), axis, 0, 0, tiled=True)
    return jnp.sum(blocks.astype(jnp.float32), axis=0)


def rms_scale(values, gain):
    widened = values.astype(jnp.float32)
    return widened * lax.rsqrt(jnp.mean(widened * widened, axis=-1, keepdims=True) + EPSILON) * gain


def slot_tables(route_block, experts, capacity):
    rows_here, top_picks = route_block.shape
    flat_routes = route_block.reshape(-1)
    onehot = (flat_routes[:, None] == jnp.arange(experts, dtype=jnp.int32)[None, :]).astype(
        jnp.int32
    )
    earlier = jnp.cumsum(onehot, axis=0) - onehot
    position = jnp.sum(earlier * onehot, axis=1)
    source_row = jnp.full((experts * capacity,), rows_here, jnp.int32)
    source_row = source_row.at[flat_routes * capacity + position].set(
        jnp.arange(rows_here * top_picks, dtype=jnp.int32) // top_picks
    )
    return (position.reshape(rows_here, top_picks), source_row)


def fold_update(grouped, query_pos, query_gate, key_block, key_gate, key_pos, running):
    running_max, row_total, summed = running
    scores = jnp.einsum(
        "tgrd,ngd->grtn", grouped, key_block[:, :, 0], preferred_element_type=jnp.float32
    ) * HEAD ** (-0.5)
    scores = scores + query_gate[..., None] - key_gate[:, :, None, :]
    causal = key_pos[None, :] <= query_pos[:, None]
    scores = jnp.where(causal, scores, NEGATIVE)
    new_max = jnp.maximum(running_max, jnp.max(scores, axis=-1))
    factor = jnp.exp(running_max - new_max)
    weight = jnp.where(causal, jnp.exp(scores - new_max[..., None]), 0.0)
    row_total = row_total * factor + jnp.sum(weight, axis=-1)
    summed = summed * factor[..., None] + jnp.einsum(
        "grtn,ngd->grtd",
        weight.astype(jnp.bfloat16),
        key_block[:, :, 1],
        preferred_element_type=jnp.float32,
    )
    return (new_max, row_total, summed)


def keep_state(running):
    return running


def gated_hidden(slot_rows, router_feature_lanes, up_columns):
    return (
        jax.nn.silu(jnp.dot(slot_rows, router_feature_lanes, preferred_element_type=jnp.float32))
        * jnp.dot(slot_rows, up_columns, preferred_element_type=jnp.float32)
    ).astype(jnp.bfloat16)


def body(
    queries,
    keys_values,
    log_gate_cum,
    mix_weight,
    mix_gain,
    moe_in,
    moe_gain,
    routes,
    route_weight,
    expert_gate,
    expert_up,
    expert_down,
):
    ep_count = lax.axis_size("ep")
    ep_index = lax.axis_index("ep")
    local_tokens = queries.shape[0]
    half_rows = local_tokens // 2
    offset = ep_index * local_tokens
    kv_local = keys_values.shape[1] // (2 * HEAD)
    heads_local = queries.shape[1] // HEAD
    group_size = heads_local // kv_local
    second_rows = queries[half_rows:]
    second_start = offset + half_rows

    def half_setup(rows, first_pos):
        grouped = rows.reshape(half_rows, kv_local, group_size, HEAD)
        query_pos = first_pos + jnp.arange(half_rows, dtype=jnp.int32)
        query_gate = lax.dynamic_slice_in_dim(log_gate_cum, first_pos, half_rows, 1)
        query_gate = query_gate.reshape(kv_local, group_size, half_rows)
        return (grouped, query_pos, query_gate, first_pos + half_rows - 1)

    halves = (half_setup(queries[:half_rows], offset), half_setup(second_rows, second_start))
    start_state = (
        jnp.full((kv_local, group_size, half_rows), NEGATIVE, jnp.float32),
        jnp.zeros((kv_local, group_size, half_rows), jnp.float32),
        jnp.zeros((kv_local, group_size, half_rows, HEAD), jnp.float32),
    )
    piece = lax.all_gather(keys_values, "ep", axis=0, tiled=True)
    piece_rows = piece.shape[0]
    block_rows = math.gcd(piece_rows, 512)

    def one_block(turn_index, fold_state):
        tile_opening = turn_index * block_rows
        key_block = lax.dynamic_slice_in_dim(piece, turn_index * block_rows, block_rows, 0)
        key_block = key_block.reshape(block_rows, kv_local, 2, HEAD)
        key_gate = lax.dynamic_slice_in_dim(log_gate_cum, tile_opening, block_rows, 1)
        key_gate = key_gate.reshape(kv_local, group_size, block_rows)
        key_pos = tile_opening + jnp.arange(block_rows, dtype=jnp.int32)
        updated = []
        for half_state, half_data in zip(fold_state, halves):
            grouped, query_pos, query_gate, last_query = half_data
            advance = partial(
                fold_update, grouped, query_pos, query_gate, key_block, key_gate, key_pos
            )
            updated.append(lax.cond(tile_opening <= last_query, advance, keep_state, half_state))
        return tuple(updated)

    folded = lax.fori_loop(0, piece_rows // block_rows, one_block, (start_state, start_state))

    def finish(state):
        _, row_total, summed = state
        mixed_heads = jnp.transpose(summed / row_total[..., None], (2, 0, 1, 3))
        return mixed_heads.reshape(half_rows, heads_local * HEAD).astype(jnp.bfloat16)

    first_done = finish(folded[0])
    second_done = finish(folded[1])
    attended = jnp.concatenate([first_done, second_done], axis=0)
    rows_here = moe_in.shape[0]
    top_picks = routes.shape[1]
    width_here = moe_in.shape[1]
    capacity = 3 * top_picks * rows_here // (2 * ep_count)
    normed = rms_scale(moe_in, moe_gain).astype(jnp.bfloat16)
    position, source_row = slot_tables(routes, ep_count, capacity)
    zero_row = jnp.zeros((1, width_here), jnp.bfloat16)
    down_here = expert_down[0]
    padded = jnp.concatenate([normed, zero_row], axis=0)
    received_rows = lax.all_to_all(
        padded[source_row].reshape(ep_count, capacity, width_here),
        "ep",
        split_axis=0,
        concat_axis=0,
        tiled=True,
    )
    slot_rows = received_rows.reshape(-1, width_here)
    slot_count = slot_rows.shape[0]
    pieces = sent_together((expert_gate[0], expert_up[0]), "tp", 1, 0)
    columns = gated_hidden(slot_rows, pieces[0], pieces[1])
    hidden = columns
    shard_rows = down_here.shape[0]
    total = jnp.zeros((slot_count, width_here), jnp.float32)
    add_piece = lax.all_gather(down_here, "tp", axis=0, tiled=True)
    for part_index in range(add_piece.shape[0] // shard_rows):
        columns = lax.dynamic_slice_in_dim(hidden, part_index * shard_rows, shard_rows, 1)
        width_part = jnp.dot(
            columns,
            add_piece[part_index * shard_rows : (part_index + 1) * shard_rows],
            preferred_element_type=jnp.float32,
        ).astype(jnp.bfloat16)
        total = total + lax.optimization_barrier(width_part).astype(jnp.float32)
    mix_sum = sum_at_owner(
        jnp.dot(attended, mix_weight, preferred_element_type=jnp.float32).astype(jnp.bfloat16),
        "tp",
        0,
    )
    mix_result = rms_scale(mix_sum, mix_gain).astype(jnp.bfloat16)
    expert_out = total.astype(jnp.bfloat16).reshape(ep_count, capacity, width_here)
    returned = lax.all_to_all(expert_out, "ep", split_axis=0, concat_axis=0, tiled=True).reshape(
        -1, width_here
    )
    chosen = returned[routes * capacity + position].astype(jnp.float32)
    moe_result = jnp.sum(route_weight[..., None] * chosen, axis=1).astype(jnp.bfloat16)
    return (mix_result, moe_result)


def solution(mesh):
    in_specs = (
        P("ep", "tp"),
        P("ep", "tp"),
        P("tp", None),
        P("tp", None),
        P(),
        P(("ep", "tp"), None),
        P(),
        P(("ep", "tp"), None),
        P(("ep", "tp"), None),
        P("ep", None, "tp"),
        P("ep", None, "tp"),
        P("ep", "tp", None),
    )
    out_specs = (P(("ep", "tp"), None), P(("ep", "tp"), None))
    return jax.shard_map(body, mesh=mesh, in_specs=in_specs, out_specs=out_specs, check_vma=False)
```

profile of v0, /device:TPU:1, one launch (start us, length us, event | category | flops | bytes accessed | tf_op | source)
XLA Modules:
  0.0 432.0 jit_solution(6988388845810025576)
XLA Ops:
  7.2 1.7 copy.22
  9.0 3.1 pad_maximum_fusion
  12.5 0.9 reduce-window.6
  14.7 2.9 scatter_custom_fusion
  17.7 4.1 gather_fusion
  21.8 4.6 %reshape.184 = bf16[64,9,2048]{2,1,0:T(8,128)(2,1)} reshape(bf16[576,2048]{1,0:T(8,128)(2,1)} %gather_fusion) | data formatting | bytes 4718592 | tf_op jit(solution)/shard_map/reshape | solution.py:166
  26.4 13.3 %all-to-all-start.1 = ((bf16[64,9,2048]{2,1,0:T(8,128)(2,1)}), bf16[64,9,2048]{2,1,0:T(8,128)(2,1)}, u32[]{:S(2)}, u32[]{:S(2)}) async-start(bf16[64,9,2048]{2,1,0:T(8,128)(2,1)} %reshape.184), calls=%async_computation.1 | async-start | bytes 8388608 | tf_op jit(solution)/shard_map/all_to_all | solution.py:165
  41.4 103.3 %all-to-all-done.1 = bf16[64,9,2048]{2,1,0:T(8,128)(2,1)} async-done(((bf16[64,9,2048]{2,1,0:T(8,128)(2,1)}), bf16[64,9,2048]{2,1,0:T(8,128)(2,1)}, u32[]{:S(2)}, u32[]{:S(2)}) %all-to-all-start.1) | async-done | bytes 2359328 | tf_op jit(solution)/shard_map/all_to_all | solution.py:165
  144.7 4.8 %reshape.185 = bf16[576,2048]{1,0:T(8,128)(2,1)} reshape(bf16[64,9,2048]{2,1,0:T(8,128)(2,1)} %all-to-all-done.1) | data formatting | bytes 4718592 | tf_op jit(solution)/shard_map/reshape | solution.py:172
  149.6 56.5 %while.24 = (s32[]{:T(128)}, f32[1,4,128]{2,1,0:T(4,128)S(1)}, f32[1,4,128]{2,1,0:T(4,128)S(1)}, f32[1,4,128,64]{2,3,1,0:T(8,128)S(1)}, f32[1,4,128]{2,1,0:T(4,1...) while((s32[]{:T(128)}, f32[1,4,128]{2,1,0:T(4,128)S(1)}, ...), condition=%wide.region_9.10_spmd.clone, body=%wide.region_0.9_spmd.clone.sunk | while | flops 140250880 | bytes 8108587 | solution.py:146
  149.6 0.9 constant_dynamic-slice_fusion.6
  151.3 1.2 conditional.7
  152.5 1.2 conditional.6
  153.7 0.9 constant_dynamic-slice_fusion.6
  155.4 0.9 constant_dynamic-slice_fusion.6
  157.1 0.9 constant_dynamic-slice_fusion.6
  158.8 0.9 constant_dynamic-slice_fusion.6
  160.5 0.9 constant_dynamic-slice_fusion.6
  162.2 0.9 constant_dynamic-slice_fusion.6
  163.8 0.9 constant_dynamic-slice_fusion.6
  165.5 0.9 constant_dynamic-slice_fusion.6
  167.2 0.9 constant_dynamic-slice_fusion.6
  168.9 0.9 constant_dynamic-slice_fusion.6
  170.6 0.9 constant_dynamic-slice_fusion.6
  172.3 0.9 constant_dynamic-slice_fusion.6
  174.0 0.9 constant_dynamic-slice_fusion.6
  175.7 0.9 constant_dynamic-slice_fusion.6
  177.4 0.9 constant_dynamic-slice_fusion.6
  179.1 0.9 constant_dynamic-slice_fusion.6
  180.8 0.9 constant_dynamic-slice_fusion.6
  182.4 0.9 constant_dynamic-slice_fusion.6
  184.1 0.9 constant_dynamic-slice_fusion.6
  185.8 0.9 constant_dynamic-slice_fusion.6
  187.5 0.9 constant_dynamic-slice_fusion.6
  189.2 0.9 constant_dynamic-slice_fusion.6
  190.9 0.9 constant_dynamic-slice_fusion.6
  192.6 0.9 constant_dynamic-slice_fusion.6
  194.3 0.9 constant_dynamic-slice_fusion.6
  196.0 0.9 constant_dynamic-slice_fusion.6
  197.7 0.9 constant_dynamic-slice_fusion.6
  199.3 0.9 constant_dynamic-slice_fusion.6
  201.0 0.9 constant_dynamic-slice_fusion.6
  202.7 0.9 constant_dynamic-slice_fusion.6
  204.4 0.9 constant_dynamic-slice_fusion.6
  206.2 1.4 convolution_convert_fusion.4
  207.6 4.7 %all-to-all-start = ((bf16[4,64,2048]{2,1,0:T(8,128)(2,1)}), bf16[4,64,2048]{2,1,0:T(8,128)(2,1)S(1)}, u32[]{:S(2)}, u32[]{:S(2)}) async-start(bf16[4,64,2048]{2,1,0:T(8,128)(2,1)} %bitcast.34), calls=%async_computation | async-start | bytes 2097152 | tf_op jit(solution)/shard_map/all_to_all | solution.py:32
  212.3 8.7 %all-gather.7.cloned.1.call-done = bf16[4096,1024]{1,0:T(8,128)(2,1)} async-done(((bf16[4096,256]{1,0:T(8,128)(2,1)}), bf16[4096,1024]{1,0:T(8,128)(2,1)}) %all-gather.7.cloned.1.call-update) | async-done | bytes 8388624 | tf_op jit(solution)/shard_map/all_gather | solution.py:22
  221.0 4.5 %fusion.44 = f32[576,1024]{1,0:T(8,128)S(1)} fusion(bf16[576,2048]{1,0:T(8,128)(2,1)S(1)} %copy-done.5, bf16[4096,1024]{1,0:T(8,128)(2,1)} %all-gather.7.cloned.1.call-done), kind=kOutput, calls=%fused_computation.63 | convolution fusion | flops 2415919104 | bytes 8912896 | tf_op jit(solution)/shard_map/dot_general | solution.py:83
  225.7 3.8 multiply_convert_fusion
  229.4 43.6 %all-gather.9.cloned.1.call-done = bf16[1,1024,2048]{2,1,0:T(8,128)(2,1)} async-done(((bf16[1,256,2048]{2,1,0:T(8,128)(2,1)}), bf16[1,1024,2048]{2,1,0:T(8,128)(2,1)}) %all-gather.9.cloned.1.call-update) | async-done | bytes 4194320 | tf_op jit(solution)/shard_map/all_gather | solution.py:179
  273.1 2.2 convolution_convert_fusion.3
  275.3 2.0 convolution_convert_fusion.2
  278.2 0.8 convolution_convert_fusion
  278.9 2.1 add_convert_fusion
  281.1 2.8 reshape.186
  283.9 1.0 copy-done.3
  284.9 26.8 %all-to-all-start.2 = ((bf16[64,9,2048]{2,1,0:T(8,128)(2,1)}), bf16[64,9,2048]{2,1,0:T(8,128)(2,1)}, u32[]{:S(2)}, u32[]{:S(2)}) async-start(bf16[64,9,2048]{2,1,0:T(8,128)(2,1)} %reshape.186), calls=%async_computation.2 | async-start | bytes 8388608 | tf_op jit(solution)/shard_map/all_to_all | solution.py:195
  312.0 1.4 convert_reduce_fusion
  313.6 0.8 multiply_convert_fusion.1
  314.4 92.0 %all-to-all-done.2 = bf16[64,9,2048]{2,1,0:T(8,128)(2,1)} async-done(((bf16[64,9,2048]{2,1,0:T(8,128)(2,1)}), bf16[64,9,2048]{2,1,0:T(8,128)(2,1)}, u32[]{:S(2)}, u32[]{:S(2)}) %all-to-all-start.2) | async-done | bytes 2359328 | tf_op jit(solution)/shard_map/all_to_all | solution.py:195
  406.4 3.4 reshape.187
  409.8 3.1 gather_fusion.1
  412.9 4.8 %reshape.221 = f32[192,2,2048]{2,1,0:T(2,128)} reshape(bf16[384,2048]{1,0:T(8,128)(2,1)} %gather_fusion.1) | data formatting | bytes 4718592 | tf_op jit(solution)/shard_map/convert_element_type | solution.py:198
  417.8 7.8 %multiply_reduce_fusion = bf16[192,2048]{1,0:T(8,128)(2,1)} fusion(f32[192,2,2048]{2,1,0:T(2,128)} %reshape.221, f32[192,2]{1,0:T(8,128)S(1)} %copy.25), kind=kLoop, calls=%fused_computation.65 | loop fusion | flops 1179648 | bytes 3933696 | tf_op jit(solution)/shard_map/reduce_sum | solution.py:199
  (274 shorter events, 30.4 us)
Async XLA Ops:
  7.2 199.0 %copy-start = (bf16[256,2048]{1,0:T(8,128)(2,1)S(1)}, bf16[256,2048]{1,0:T(8,128)(2,1)}, u32[]{:S(2)}) copy-start(bf16[256,2048]{1,0:T(8,128)(2,1)} %param.21) | copy-start | bytes 3145732
  7.2 142.4 %all-gather.5.cloned.1.call-start = ((), (), s32[]{:S(2)}) async-start(), calls=%async_computation.3 | async-start | bytes 4259840 | tf_op jit(solution)/shard_map/all_gather | solution.py:126
  8.9 212.1 %all-gather.7.cloned.1.call-start = ((), (), s32[]{:S(2)}) async-start(), calls=%async_computation.4 | async-start | bytes 10485760 | tf_op jit(solution)/shard_map/all_gather | solution.py:22
  9.0 3.1 copy-start.10
  12.0 2.1 copy-start.4
  12.0 2.3 copy-start.8
  26.4 14.1 %copy-start.7 = (bf16[256,256]{1,0:T(8,128)(2,1)S(1)}, bf16[256,256]{1,0:T(8,128)(2,1)}, u32[]{:S(2)}) copy-start(bf16[256,256]{1,0:T(8,128)(2,1)} %param.18) | copy-start | bytes 393220
  26.4 118.3 %all-to-all-start.1 = ((bf16[64,9,2048]{2,1,0:T(8,128)(2,1)}), bf16[64,9,2048]{2,1,0:T(8,128)(2,1)}, u32[]{:S(2)}, u32[]{:S(2)}) async-start(bf16[64,9,2048]{2,1,0:T(8,128)(2,1)} %reshape.184), calls=%async_computation.1 | async-start | bytes 8388608 | tf_op jit(solution)/shard_map/all_to_all | solution.py:165
  39.7 233.4 %all-gather.9.cloned.1.call-start = ((), (), s32[]{:S(2)}) async-start(), calls=%async_computation.5 | async-start | bytes 5242880 | tf_op jit(solution)/shard_map/all_gather | solution.py:179
  206.2 14.9 %copy-start.5 = (bf16[576,2048]{1,0:T(8,128)(2,1)S(1)}, bf16[576,2048]{1,0:T(8,128)(2,1)}, u32[]{:S(2)}) copy-start(bf16[576,2048]{1,0:T(8,128)(2,1)} %reshape.185) | copy-start | bytes 7077892
  207.6 76.3 %all-to-all-start = ((bf16[4,64,2048]{2,1,0:T(8,128)(2,1)}), bf16[4,64,2048]{2,1,0:T(8,128)(2,1)S(1)}, u32[]{:S(2)}, u32[]{:S(2)}) async-start(bf16[4,64,2048]{2,1,0:T(8,128)(2,1)} %bitcast.34), calls=%async_computation | async-start | bytes 2097152 | tf_op jit(solution)/shard_map/all_to_all | solution.py:32
  221.0 4.6 %copy-start.12 = (bf16[4096,1024]{1,0:T(8,128)(2,1)S(1)}, bf16[4096,1024]{1,0:T(8,128)(2,1)}, u32[]{:S(2)}) copy-start(bf16[4096,1024]{1,0:T(8,128)(2,1)} %all-gather.7.cloned.1.call-done) | copy-start | bytes 25165828
  229.4 45.9 %copy-start.6 = (bf16[576,1024]{1,0:T(8,128)(2,1)S(1)}, bf16[576,1024]{1,0:T(8,128)(2,1)}, u32[]{:S(2)}) copy-start(bf16[576,1024]{1,0:T(8,128)(2,1)} %multiply_convert_fusion) | copy-start | bytes 3538948
  273.1 4.3 copy-start.2
  283.9 28.0 %copy-start.11 = (f32[192,2]{0,1:T(2,128)S(1)}, f32[192,2]{0,1:T(2,128)}, u32[]{:S(2)}) copy-start(f32[192,2]{0,1:T(2,128)} %param.26) | copy-start | bytes 4612
  283.9 29.7 %copy-start.9 = (f32[2048]{0:T(1024)S(1)}, f32[2048]{0:T(1024)}, u32[]{:S(2)}) copy-start(f32[2048]{0:T(1024)} %param.22) | copy-start | bytes 24580
  283.9 1.1 copy-start.3
  284.9 121.5 %all-to-all-start.2 = ((bf16[64,9,2048]{2,1,0:T(8,128)(2,1)}), bf16[64,9,2048]{2,1,0:T(8,128)(2,1)}, u32[]{:S(2)}, u32[]{:S(2)}) async-start(bf16[64,9,2048]{2,1,0:T(8,128)(2,1)} %reshape.186), calls=%async_computation.2 | async-start | bytes 8388608 | tf_op jit(solution)/shard_map/all_to_all | solution.py:195
  412.9 12.6 %copy-start.1 = (bf16[256,2048]{1,0:T(8,128)(2,1)S(1)}, bf16[256,2048]{1,0:T(8,128)(2,1)}, u32[]{:S(2)}) copy-start(bf16[256,2048]{1,0:T(8,128)(2,1)} %param.21) | copy-start | bytes 3145732
Sparse Core Ops, SparseCore 0:
  11.2 118.5 all-gather.4
  131.6 89.3 all-gather.6
  222.8 50.1 all-gather.8
where the time goes:
time: 436 us; the launch traced here: 432 us
  waiting for transfers between devices  248 us (57%)
  local copies, waits for them, and re-layouts  87.8 us (20%)
  starting transfers between devices  44.9 us (10%)
  other arithmetic  17.9 us (4%)
  matrix products  17.1 us (4%)
  between operations  14.1 us (3%)
    all_to_all x1, waiting for transfers between devices, body(): lax.all_to_all(padded[source_row].reshape(ep_count, capacity, width_here)...  103 us
    all_to_all x1, waiting for transfers between devices, body(): lax.all_to_all(expert_out, 'ep', split_axis=0, concat_axis=0, tiled=True)  92 us
    all_gather x1, waiting for transfers between devices, body(): add_piece = lax.all_gather(down_here, 'tp', axis=0, tiled=True)  43.6 us
    dynamic_slice x32, local copies, waits for them, and re-layouts, one_block(): lax.dynamic_slice_in_dim(piece, turn_index * block_rows, block_rows, 0)  29.5 us
    all_to_all x1, starting transfers between devices, body(): lax.all_to_all(expert_out, 'ep', split_axis=0, concat_axis=0, tiled=True)  26.8 us
    dynamic_slice x32, local copies, waits for them, and re-layouts, one_block(): lax.dynamic_slice_in_dim(log_gate_cum, tile_opening, block_rows, 1)  22.6 us
    all_to_all x1, starting transfers between devices, body(): lax.all_to_all(padded[source_row].reshape(ep_count, capacity, width_here)...  13.3 us
  transfers between devices with their start and end apart: 6, of which 4 were waited for; matrix products, arithmetic and copies ran while one was open for 23% of the time, Pallas kernels for 0%

commit v1 on v0

v1 whole, which is shorter than its diff:
```python
import functools

import jax
import jax.numpy as jnp
from jax import lax
from jax.experimental import pallas as pl
from jax.experimental.pallas import tpu as pltpu
from jax.sharding import PartitionSpec as P

HEAD = 64
EPSILON = 1e-06
NEGATIVE = -3e38
LANES = 128
KEY_BLOCK = 512
MESH = pl.DeviceIdType.MESH
F32 = jnp.float32
BF16 = jnp.bfloat16


def dot(a, b):
    return jnp.dot(a, b, preferred_element_type=F32)


def rms_scale(values, gain):
    return values * lax.rsqrt(jnp.mean(values * values, axis=-1, keepdims=True) + EPSILON) * gain


def pack_kernel(capacity, x_ref, gain_ref, routes_ref, out_ref, wide):
    rows, width = x_ref.shape
    tiles = width // LANES
    slots = out_ref.shape[0] // tiles
    experts = slots // capacity
    normed = rms_scale(x_ref[...].astype(F32), gain_ref[...]).astype(BF16)
    ids = lax.broadcasted_iota(jnp.int32, (experts, rows), 0)
    first = (ids == routes_ref[0:1, :]).astype(F32)
    second = (ids == routes_ref[1:2, :]).astype(F32)
    upper = (
        lax.broadcasted_iota(jnp.int32, (rows, rows), 0)
        < lax.broadcasted_iota(jnp.int32, (rows, rows), 1)
    ).astype(BF16)
    first_before = dot(first.astype(BF16), upper)
    second_before = dot(second.astype(BF16), upper) + jnp.sum(first, axis=1, keepdims=True)
    first_pos = jnp.sum(first * first_before, axis=0, keepdims=True).astype(jnp.int32)
    second_pos = jnp.sum(second * second_before, axis=0, keepdims=True).astype(jnp.int32)
    slot_ids = lax.broadcasted_iota(jnp.int32, (slots, rows), 0)
    pick = jnp.where(
        (slot_ids == routes_ref[0:1, :] * capacity + first_pos)
        | (slot_ids == routes_ref[1:2, :] * capacity + second_pos),
        1.0,
        0.0,
    ).astype(BF16)
    for half in range(tiles // 2):
        moved = dot(pick, normed[:, half * 2 * LANES : (half + 1) * 2 * LANES])
        wide[pl.ds(2 * half, slots, stride=tiles), :] = moved[:, :LANES]
        wide[pl.ds(2 * half + 1, slots, stride=tiles), :] = moved[:, LANES:]
    out_ref[...] = wide[...].astype(BF16)


def unpack_kernel(
    capacity, ret_ref, routes_ref, weight_ref, mix_ref, gain_ref, mix_out, moe_out, wide
):
    rows, width = moe_out.shape
    tiles = width // LANES
    slots = ret_ref.shape[0] // tiles
    experts = slots // capacity
    wide[...] = ret_ref[...].astype(F32)
    ids = lax.broadcasted_iota(jnp.int32, (rows, experts), 1)
    first = (ids == routes_ref[:, 0:1]).astype(F32)
    second = (ids == routes_ref[:, 1:2]).astype(F32)
    lower = (
        lax.broadcasted_iota(jnp.int32, (rows, rows), 1)
        < lax.broadcasted_iota(jnp.int32, (rows, rows), 0)
    ).astype(BF16)
    first_before = dot(lower, first.astype(BF16))
    second_before = dot(lower, second.astype(BF16)) + jnp.sum(first, axis=0, keepdims=True)
    first_pos = jnp.sum(first * first_before, axis=1, keepdims=True).astype(jnp.int32)
    second_pos = jnp.sum(second * second_before, axis=1, keepdims=True).astype(jnp.int32)
    slot_ids = lax.broadcasted_iota(jnp.int32, (rows, slots), 1)
    first_pick = jnp.where(
        slot_ids == routes_ref[:, 0:1] * capacity + first_pos, 1.0, 0.0
    ).astype(BF16)
    second_pick = jnp.where(
        slot_ids == routes_ref[:, 1:2] * capacity + second_pos, 1.0, 0.0
    ).astype(BF16)
    for half in range(tiles // 2):
        block = jnp.concatenate(
            [wide[pl.ds(2 * half + side, slots, stride=tiles), :] for side in (0, 1)], axis=1
        ).astype(BF16)
        total = weight_ref[:, 0:1] * dot(first_pick, block)
        total = total + weight_ref[:, 1:2] * dot(second_pick, block)
        moe_out[:, half * 2 * LANES : (half + 1) * 2 * LANES] = total.astype(BF16)
    summed = mix_ref[0].astype(F32)
    for part in range(1, mix_ref.shape[0]):
        summed = summed + mix_ref[part].astype(F32)
    mix_out[...] = rms_scale(summed, gain_ref[...]).astype(BF16)


def main_kernel(
    planes,
    columns,
    send_ref,
    q_ref,
    kv_ref,
    gate_log_ref,
    mixw_ref,
    gate_ref,
    up_ref,
    down_ref,
    ret_ref,
    mixr_ref,
    wg,
    wu,
    wd,
    kvb,
    recv,
    xs,
    hid,
    wide,
    outb,
    qs,
    m_ref,
    l_ref,
    acc_ref,
    mixb,
    own_sem,
    wsend,
    wrecv,
    kzsend,
    kzrecv,
    kxsend,
    kxrecv,
    kcsend,
    kcrecv,
    dsend,
    drecv,
    csend,
    crecv,
    msend,
    mrecv,
):
    ep = planes * columns * 2
    tp = 4
    me = lax.axis_index("ep")
    my = lax.axis_index("tp")
    my_z = me // (2 * columns)
    my_x = (me // 2) % columns
    my_c = me % 2
    right, left = (my + 1) % tp, (my + 3) % tp
    far = (my + 2) % tp
    chunk = send_ref.shape[0] // ep
    queries = q_ref.shape[0]
    heads = q_ref.shape[1] // HEAD
    model = down_ref.shape[1]
    tiles = model // LANES

    def at(e, t=None):
        return {"ep": e, "tp": my if t is None else t}

    barrier = pltpu.get_barrier_semaphore()

    def greet_ep(k, carry):
        pl.semaphore_signal(barrier, inc=1, device_id=at((me + k) % ep), device_id_type=MESH)
        return carry

    lax.fori_loop(1, ep, greet_ep, 0)
    for k in range(1, tp):
        pl.semaphore_signal(barrier, inc=1, device_id=at(me, (my + k) % tp), device_id_type=MESH)
    pl.semaphore_wait(barrier, ep - 1 + tp - 1)

    def remote(src, dst, s_sem, r_sem, where):
        return pltpu.make_async_remote_copy(
            src_ref=src, dst_ref=dst, send_sem=s_sem, recv_sem=r_sem, device_id=where,
            device_id_type=MESH,
        )

    mats = ((gate_ref, wg), (up_ref, wu), (down_ref, wd))
    near = {}
    for m, (src, dst) in enumerate(mats):
        for way, peer in enumerate((right, left)):
            near[m, way] = remote(
                src, dst.at[my], wsend.at[way, m, 0], wrecv.at[way, m, 0], at(me, peer)
            )
            near[m, way].start()

    def kv_slot(z, x, c):
        return (z * columns + x) * 2 + c

    def z_copy(k):
        z = (my_z + k) % planes
        return remote(
            kv_ref, kvb.at[me], kzsend.at[k], kzrecv.at[k], at(kv_slot(z, my_x, my_c))
        )

    for k in range(1, planes):
        z_copy(k).start()

    def dispatch(k):
        e = (me + k) % ep
        return remote(
            send_ref.at[pl.ds(pl.multiple_of(e * chunk, 16), chunk)],
            recv.at[pl.ds(pl.multiple_of(me * chunk, 16), chunk)],
            dsend.at[k],
            drecv.at[k],
            at(e),
        )

    def start_dispatch(k, carry):
        dispatch(k).start()
        return carry

    lax.fori_loop(1, ep, start_dispatch, 0)

    own = [
        pltpu.make_async_copy(src, dst.at[my], own_sem.at[m]) for m, (src, dst) in enumerate(mats)
    ]
    for copy in own:
        copy.start()
    kvb[me] = kv_ref[...]
    mine = pl.ds(pl.multiple_of(me * chunk, 16), chunk)
    recv[mine, :] = send_ref[mine, :]

    for h in range(heads):
        part = q_ref[:, h * HEAD : (h + 1) * HEAD].astype(F32) * HEAD ** (-0.5)
        qs[h] = jnp.concatenate([part, jnp.zeros_like(part)], axis=1).astype(BF16)
        m_ref[h] = jnp.full((queries, LANES), NEGATIVE, F32)
        l_ref[h] = jnp.zeros((queries, LANES), F32)
        acc_ref[h] = jnp.zeros((queries, LANES), F32)

    def x_copy(k, j):
        slab = kvb.at[kv_slot((my_z + planes - j) % planes, my_x, my_c)]
        return remote(
            slab,
            slab,
            kxsend.at[k * planes + j],
            kxrecv.at[k * planes + j],
            at(kv_slot(my_z, (my_x + k) % columns, my_c)),
        )

    def c_copy(k, j):
        slab = kvb.at[kv_slot((my_z + planes - j) % planes, (my_x + columns - k) % columns, my_c)]
        return remote(
            slab, slab, kcsend.at[k * planes + j], kcrecv.at[k * planes + j], at(me + 1 - 2 * my_c)
        )

    for j in range(planes):
        if j > 0:
            z_copy(j).wait_recv()
        for k in range(1, columns):
            x_copy(k, j).start()
        c_copy(0, j).start()

    def pass_on(j, carry):
        for k in range(1, columns):
            x_copy(k, j).wait_recv()
            c_copy(k, j).start()
        return carry

    lax.fori_loop(0, planes, pass_on, 0)

    def far_copy(m, way):
        dst = mats[m][1]
        source = left if way == 0 else right
        peer = right if way == 0 else left
        half = dst.shape[1] // 2
        block = dst.at[source, pl.ds(way * half, half)]
        return remote(block, block, wsend.at[way, m, 1], wrecv.at[way, m, 1], at(me, peer))

    for m in (0, 1):
        for way in (0, 1):
            near[m, way].wait_recv()
            far_copy(m, way).start()

    def wait_c(j, carry):
        c_copy(0, j).wait_recv()
        for k in range(1, columns):
            c_copy(k, j).wait_recv()
        return carry

    lax.fori_loop(0, planes, wait_c, 0)

    base = gate_log_ref[:, pl.ds(pl.multiple_of(me * queries, LANES), LANES)][:, 0:1]
    slabs = KEY_BLOCK // queries

    def attend(i, masked):
        keys = kvb[pl.ds(i * slabs, slabs)].reshape(KEY_BLOCK, 2 * HEAD)
        start = pl.multiple_of(i * KEY_BLOCK, KEY_BLOCK)
        bias = base - gate_log_ref[:, pl.ds(start, KEY_BLOCK)]
        for h in range(heads):
            scores = lax.dot_general(
                qs[h], keys, (((1,), (1,)), ((), ())), preferred_element_type=F32
            )
            scores = scores + bias[h : h + 1, :]
            if masked:
                key_pos = start + lax.broadcasted_iota(jnp.int32, scores.shape, 1)
                query_pos = me * queries + lax.broadcasted_iota(jnp.int32, scores.shape, 0)
                scores = jnp.where(key_pos <= query_pos, scores, NEGATIVE)
            old = m_ref[h]
            new = jnp.maximum(old, jnp.max(scores, axis=1, keepdims=True))
            factor = jnp.exp(old - new)
            weight = jnp.exp(scores - jnp.concatenate([new] * (KEY_BLOCK // LANES), axis=1))
            part = weight[:, :LANES]
            for t in range(1, KEY_BLOCK // LANES):
                part = part + weight[:, t * LANES : (t + 1) * LANES]
            m_ref[h] = new
            l_ref[h] = l_ref[h] * factor + part
            acc_ref[h] = acc_ref[h] * factor + dot(weight.astype(BF16), keys)

    full = me // slabs

    def attend_full(i, carry):
        attend(i, False)
        return carry

    lax.fori_loop(0, full, attend_full, 0)
    attend(full, True)

    for way in (0, 1):
        near[2, way].wait_recv()
        far_copy(2, way).start()

    attended = jnp.concatenate(
        [acc_ref[h][:, HEAD:] / jnp.sum(l_ref[h], axis=1, keepdims=True) for h in range(heads)],
        axis=1,
    ).astype(BF16)
    mixb[...] = dot(attended, mixw_ref[...]).astype(BF16)
    share = queries // tp

    def mix_copy(k):
        t = (my + k) % tp
        return remote(
            mixb.at[pl.ds(pl.multiple_of(t * share, 16), share)],
            mixr_ref.at[k],
            msend.at[k],
            mrecv.at[k],
            at(me, t),
        )

    for k in range(1, tp):
        mix_copy(k).start()
    mixr_ref[0] = mixb[pl.ds(pl.multiple_of(my * share, 16), share), :]

    def wait_dispatch(k, carry):
        dispatch(k).wait_recv()
        return carry

    lax.fori_loop(1, ep, wait_dispatch, 0)
    groups = 4
    group_rows = xs.shape[0] // groups
    group_tiles = group_rows * tiles

    def spread(g, carry):
        wide[...] = recv[pl.ds(pl.multiple_of(g * group_tiles, 16), group_tiles), :].astype(F32)
        rows = pl.ds(pl.multiple_of(g * group_rows, 16), group_rows)
        for j in range(tiles):
            xs[rows, j * LANES : (j + 1) * LANES] = wide[
                pl.ds(j, group_rows, stride=tiles), :
            ].astype(BF16)
        return carry

    lax.fori_loop(0, groups, spread, 0)

    for copy in own:
        copy.wait()

    def expand(q):
        up_part = dot(xs[...], wu[q])
        gate_part = dot(xs[...], wg[q])
        hid[q] = (gate_part / (1.0 + jnp.exp(-gate_part)) * up_part).astype(BF16)

    for m in (0, 1):
        for way in (0, 1):
            far_copy(m, way).wait_recv()

    def expand_step(q, carry):
        expand(q)
        return carry

    lax.fori_loop(0, tp, expand_step, 0)
    for way in (0, 1):
        far_copy(2, way).wait_recv()

    per_group = ep // groups
    cols = 4 * LANES

    def combine(s, k):
        return remote(
            outb.at[pl.ds(pl.multiple_of(s * chunk, 16), chunk)],
            ret_ref.at[pl.ds(pl.multiple_of(me * chunk, 16), chunk)],
            csend.at[k],
            crecv.at[k],
            at(s),
        )

    def contract(i, carry):
        g = (i + me // per_group) % groups
        rows = pl.ds(pl.multiple_of(g * group_rows, 16), group_rows)
        for n in range(model // cols):
            total = jnp.zeros((group_rows, cols), F32)
            for q in range(tp):
                total = total + dot(hid[q, rows, :], wd[q, :, n * cols : (n + 1) * cols])
            for j in range(4):
                wide[pl.ds(n * 4 + j, group_rows, stride=tiles), :] = total[
                    :, j * LANES : (j + 1) * LANES
                ]
        outb[pl.ds(pl.multiple_of(g * group_tiles, 16), group_tiles), :] = wide[...].astype(BF16)

        def start_combine(j, carry):
            s = g * per_group + (j + me) % per_group

            @pl.when(s != me)
            def _():
                combine(s, (s + ep - me) % ep).start()

            return carry

        lax.fori_loop(0, per_group, start_combine, 0)
        return carry

    lax.fori_loop(0, groups, contract, 0)
    ret_ref[mine, :] = outb[mine, :]

    for k in range(1, tp):
        mix_copy(k).wait()

    def wait_combine(k, carry):
        combine((me + k) % ep, k).wait()
        dispatch(k).wait_send()
        return carry

    lax.fori_loop(1, ep, wait_combine, 0)
    for k in range(1, planes):
        z_copy(k).wait_send()

    def wait_kv(j, carry):
        c_copy(0, j).wait_send()
        for k in range(1, columns):
            x_copy(k, j).wait_send()
            c_copy(k, j).wait_send()
        return carry

    lax.fori_loop(0, planes, wait_kv, 0)
    for m in range(3):
        for way in (0, 1):
            near[m, way].wait_send()
            far_copy(m, way).wait_send()


def body(
    planes,
    columns,
    queries,
    keys_values,
    log_gate_cum,
    mix_weight,
    mix_gain,
    moe_in,
    moe_gain,
    routes,
    route_weight,
    expert_gate,
    expert_up,
    expert_down,
):
    ep = planes * columns * 2
    tp = 4
    tokens, model = moe_in.shape
    tiles = model // LANES
    capacity = 3 * routes.shape[1] * tokens // (2 * ep)
    slots = ep * capacity
    rows = queries.shape[0]
    heads = queries.shape[1] // HEAD
    depth, width = expert_gate.shape[1:]
    vmem = pl.BlockSpec(memory_space=pltpu.VMEM)
    hbm = pl.BlockSpec(memory_space=pl.ANY)
    big = 64000 * 1024

    packed = pl.pallas_call(
        functools.partial(pack_kernel, capacity),
        out_shape=jax.ShapeDtypeStruct((slots * tiles, LANES), BF16),
        in_specs=[vmem] * 3,
        out_specs=vmem,
        scratch_shapes=[pltpu.VMEM((slots * tiles, LANES), F32)],
        compiler_params=pltpu.CompilerParams(vmem_limit_bytes=big // 2),
        name="pack",
    )(moe_in, moe_gain[None], routes.T)

    dma = pltpu.SemaphoreType.DMA
    returned, mixed = pl.pallas_call(
        functools.partial(main_kernel, planes, columns),
        out_shape=(
            jax.ShapeDtypeStruct((slots * tiles, LANES), BF16),
            jax.ShapeDtypeStruct((tp, rows // tp, model), BF16),
        ),
        in_specs=[vmem] * 5 + [hbm] * 3,
        out_specs=(vmem, vmem),
        scratch_shapes=[
            pltpu.VMEM((tp, depth, width), BF16),
            pltpu.VMEM((tp, depth, width), BF16),
            pltpu.VMEM((tp, width, model), BF16),
            pltpu.VMEM((ep, rows, 2 * HEAD), BF16),
            pltpu.VMEM((slots * tiles, LANES), BF16),
            pltpu.VMEM((slots, model), BF16),
            pltpu.VMEM((tp, slots, width), BF16),
            pltpu.VMEM((slots * tiles // 4, LANES), F32),
            pltpu.VMEM((slots * tiles, LANES), BF16),
            pltpu.VMEM((heads, rows, 2 * HEAD), BF16),
            pltpu.VMEM((heads, rows, LANES), F32),
            pltpu.VMEM((heads, rows, LANES), F32),
            pltpu.VMEM((heads, rows, LANES), F32),
            pltpu.VMEM((rows, model), BF16),
            dma((3,)),
            dma((2, 3, 2)),
            dma((2, 3, 2)),
            dma((planes,)),
            dma((planes,)),
            dma((columns * planes,)),
            dma((columns * planes,)),
            dma((columns * planes,)),
            dma((columns * planes,)),
            dma((ep,)),
            dma((ep,)),
            dma((ep,)),
            dma((ep,)),
            dma((tp,)),
            dma((tp,)),
        ],
        compiler_params=pltpu.CompilerParams(
            collective_id=0, has_side_effects=True, vmem_limit_bytes=big
        ),
        name="exchange",
    )(
        packed,
        queries,
        keys_values,
        log_gate_cum,
        mix_weight,
        expert_gate[0],
        expert_up[0],
        expert_down[0],
    )

    return pl.pallas_call(
        functools.partial(unpack_kernel, capacity),
        out_shape=(
            jax.ShapeDtypeStruct((rows // tp, model), BF16),
            jax.ShapeDtypeStruct((tokens, model), BF16),
        ),
        in_specs=[vmem] * 5,
        out_specs=(vmem, vmem),
        scratch_shapes=[pltpu.VMEM((slots * tiles, LANES), F32)],
        compiler_params=pltpu.CompilerParams(vmem_limit_bytes=big // 2),
        name="unpack",
    )(returned, routes, route_weight, mixed, mix_gain[None])


def solution(mesh, planes=8, columns=4):
    in_specs = (
        P("ep", "tp"),
        P("ep", "tp"),
        P("tp", None),
        P("tp", None),
        P(),
        P(("ep", "tp"), None),
        P(),
        P(("ep", "tp"), None),
        P(("ep", "tp"), None),
        P("ep", None, "tp"),
        P("ep", None, "tp"),
        P("ep", "tp", None),
    )
    out_specs = (P(("ep", "tp"), None), P(("ep", "tp"), None))
    return jax.shard_map(
        functools.partial(body, planes, columns),
        mesh=mesh,
        in_specs=in_specs,
        out_specs=out_specs,
        check_vma=False,
    )
```

time: 436 us -> 194 us (0.44)
  waiting for transfers between devices: 248 us -> 0 us
  Pallas kernels: 0 us -> 186 us
  local copies, waits for them, and re-layouts: 87.8 us -> 7.03 us
  starting transfers between devices: 44.9 us -> 0 us
  other arithmetic: 17.9 us -> 0 us
  matrix products: 17.1 us -> 0 us
  between operations: 14.1 us -> 0.72 us
    all_to_all x3 -> x0, waiting for transfers between devices: 195 us -> none  [the longest x1 103 us: body(): lax.all_to_all(padded[source_row].reshape(ep_count, capacity, width_here)...]
    pallas_call x0 -> x3, Pallas kernels: none -> 186 us  [the longest x1 180 us: body(): pl.pallas_call(functools.partial(main_kernel, planes, columns), out_shape...]
    dynamic_slice x65 -> x0, local copies, waits for them, and re-layouts: 52.7 us -> none  [the longest x32 29.5 us: one_block(): lax.dynamic_slice_in_dim(piece, turn_index * block_rows, block_rows, 0)]
    all_gather x3 -> x0, waiting for transfers between devices: 52.3 us -> none  [the longest x1 43.6 us: body(): add_piece = lax.all_gather(down_here, 'tp', axis=0, tiled=True)]
    all_to_all x3 -> x0, starting transfers between devices: 44.8 us -> none  [the longest x1 26.8 us: body(): lax.all_to_all(expert_out, 'ep', split_axis=0, concat_axis=0, tiled=True)]
    dot_general x11 -> x0, matrix products: 17.1 us -> none  [the longest x4 5.82 us: body(): jnp.dot(columns, add_piece[part_index * shard_rows:(part_index + 1) * sha...]
    reshape x5 -> x0, local copies, waits for them, and re-layouts: 15.8 us -> none  [the longest x1 4.84 us: body(): slot_rows = received_rows.reshape(-1, width_here)]
    reduce_sum x7 -> x0, other arithmetic: 10.1 us -> none  [the longest x1 7.76 us: body(): jnp.sum(route_weight[..., None] * chosen, axis=1).astype(jnp.bfloat16)]
  transfers between devices with their start and end apart: 6 -> 0, of which waited for: 4 -> 0; matrix products, arithmetic and copies ran while one was open for 23% -> 0% of each run, Pallas kernels for 0% -> 0%
where the time goes in v1:
time: 194 us
  Pallas kernels  186 us (96%)
  local copies, waits for them, and re-layouts  7.03 us (4%)
    pallas_call x1, Pallas kernels, body(): pl.pallas_call(functools.partial(main_kernel, planes, columns), out_shape...  180 us
    unnamed x20, local copies, waits for them, and re-layouts  7.03 us

profile of v1, /device:TPU:1, one launch (start us, length us, event | category | flops | bytes accessed | tf_op | source)
XLA Modules:
  0.0 193.9 jit_solution(13147040091283819526)
XLA Ops:
  0.6 0.0 copy-start.3
  0.6 1.1 copy-done.3
  1.8 0.0 copy-start.4
  1.8 0.7 copy-done.4
  2.5 0.0 copy-start.6
  2.5 0.7 copy-done.6
  3.1 2.1 %pack.1.send_ref = bf16[9216,128]{1,0:T(8,128)(2,1)S(1)} custom-call(bf16[192,2048]{1,0:T(8,128)(2,1)S(1)} %copy-done.3, f32[1,2048]{1,0:T(1,128)S(1)} %bitcast.6, s32[2,192]{1,0:T(2,128)S(1)} %bitcast.8), custom_call_target="tpu_custom_call" | custom-call | tf_op jit(solution)/shard_map/pack/pallas_call | solution.py:477
  5.3 0.0 copy-start
  5.3 1.4 copy-done
  6.7 0.0 copy-start.7
  6.7 0.0 copy-start.8
  6.7 0.0 copy-start.5
  6.7 180.5 %exchange.1 = (bf16[9216,128]{1,0:T(8,128)(2,1)}, bf16[4,64,2048]{2,1,0:T(8,128)(2,1)}) custom-call(bf16[9216,128]{1,0:T(8,128)(2,1)} %copy-done, bf16[256,256]{1,0:T(8,128)(2,1)} %q_ref.1, bf16[256,128]{1,0:T(8,128)(2,1)} %kv_ref.1, f32[4,16384]{1,0:T(4,128)} %gate_log_ref.1, bf16[256,2048]{1,0:T(8,128)(2,1)} %mixw_ref.1, bf16[2048,256]{1,0:T(8,128)(2,1)} %bitcast.9, ...), custom_call_target="tpu_custom_call" | custom-call | tf_op jit(solution)/shard_map/exchange/pallas_call | solution.py:488
  187.1 0.0 copy-done.7
  187.2 0.1 copy.14.routes_ref
  187.3 0.0 copy-done.8
  187.3 0.1 copy.15.weight_ref
  187.4 0.0 copy-done.5
  187.4 0.0 copy-start.1
  187.4 1.7 copy-done.1
  189.1 0.0 copy-start.2
  189.1 1.2 copy-done.2
  190.3 3.6 %unpack.1 = (bf16[64,2048]{1,0:T(8,128)(2,1)}, bf16[192,2048]{1,0:T(8,128)(2,1)}) custom-call(bf16[9216,128]{1,0:T(8,128)(2,1)S(1)} %copy-done.1, s32[192,2]{1,0:T(8,128)S(1)} %copy.14.routes_ref, f32[192,2]{1,0:T(8,128)S(1)} %copy.15.weight_ref, bf16[4,64,2048]{2,1,0:T(8,128)(2,1)S(1)} %copy-done.2, f32[1,2048]{1,0:T(1,128)S(1)} %bitcast.7), custom_call_target="tpu_custom_call" | custom-call | tf_op jit(solution)/shard_map/unpack/pallas_call | solution.py:542
Async XLA Ops:
  0.6 1.1 copy-start.3
  1.8 0.7 copy-start.4
  2.5 0.7 copy-start.6
  5.3 1.4 copy-start
  6.7 180.5 %copy-start.7 = (s32[192,2]{0,1:T(2,128)S(1)}, s32[192,2]{0,1:T(2,128)}, u32[]{:S(2)}) copy-start(s32[192,2]{0,1:T(2,128)} %param.19) | copy-start | bytes 4612
  6.7 180.6 %copy-start.8 = (f32[192,2]{0,1:T(2,128)S(1)}, f32[192,2]{0,1:T(2,128)}, u32[]{:S(2)}) copy-start(f32[192,2]{0,1:T(2,128)} %param.20) | copy-start | bytes 4612
  6.7 180.7 %copy-start.5 = (f32[2048]{0:T(1024)S(1)}, f32[2048]{0:T(1024)}, u32[]{:S(2)}) copy-start(f32[2048]{0:T(1024)} %param.16) | copy-start | bytes 24580
  187.4 1.7 copy-start.1
  189.1 1.2 copy-start.2

commit v2 on v1

v2 whole, which is shorter than its diff:
```python
import functools

import jax
import jax.numpy as jnp
from jax import lax
from jax.experimental import pallas as pl
from jax.experimental.pallas import tpu as pltpu
from jax.sharding import PartitionSpec as P

HEAD = 64
EPSILON = 1e-06
NEGATIVE = -3e38
LANES = 128
KEY_BLOCK = 512
GROUPS = 4
PIECES = (0, 32, 64, 96, 144)
MESH = pl.DeviceIdType.MESH
F32 = jnp.float32
BF16 = jnp.bfloat16


def dot(a, b):
    return jnp.dot(a, b, preferred_element_type=F32)


def rms_scale(values, gain):
    return values * lax.rsqrt(jnp.mean(values * values, axis=-1, keepdims=True) + EPSILON) * gain


def step_kernel(
    planes,
    columns,
    q_hbm,
    kv_hbm,
    gate_log_hbm,
    mixw_hbm,
    mix_gain_ref,
    x_hbm,
    moe_gain_ref,
    routes_ref,
    weight_ref,
    gate_hbm,
    up_hbm,
    down_hbm,
    mix_out,
    moe_out,
    x_ref,
    q_ref,
    gate_log_ref,
    mixw_ref,
    wg,
    wu,
    wd,
    kvb,
    picks,
    send,
    recv,
    xs,
    hid,
    wide,
    outb,
    ret,
    qs,
    m_ref,
    l_ref,
    acc_ref,
    mixb,
    mixr,
    own_sem,
    wsend,
    wrecv,
    kzsend,
    kzrecv,
    kxsend,
    kxrecv,
    kcsend,
    kcrecv,
    dsend,
    drecv,
    csend,
    crecv,
    msend,
    mrecv,
):
    ep = planes * columns * 2
    tp = 4
    me = lax.axis_index("ep")
    my = lax.axis_index("tp")
    my_z = me // (2 * columns)
    my_x = (me // 2) % columns
    my_c = me % 2
    tokens, model = x_ref.shape
    tiles = model // LANES
    slots = xs.shape[0]
    capacity = slots // ep
    chunk = capacity * tiles
    per_group = ep // GROUPS
    group_rows = slots // GROUPS
    my_group = me // per_group
    queries = q_ref.shape[0]
    heads = q_ref.shape[1] // HEAD

    def at(e, t=None):
        return {"ep": e, "tp": my if t is None else t}

    def remote(src, dst, s_sem, r_sem, where):
        return pltpu.make_async_remote_copy(
            src_ref=src,
            dst_ref=dst,
            send_sem=s_sem,
            recv_sem=r_sem,
            device_id=where,
            device_id_type=MESH,
        )

    barrier = pltpu.get_barrier_semaphore()

    def greet_ep(k, carry):
        pl.semaphore_signal(barrier, inc=1, device_id=at((me + k) % ep), device_id_type=MESH)
        return carry

    lax.fori_loop(1, ep, greet_ep, 0)
    for k in range(1, tp):
        pl.semaphore_signal(barrier, inc=1, device_id=at(me, (my + k) % tp), device_id_type=MESH)

    own = [
        pltpu.make_async_copy(src, dst, own_sem.at[i])
        for i, (src, dst) in enumerate(
            (
                (x_hbm, x_ref),
                (kv_hbm, kvb.at[me]),
                (q_hbm, q_ref),
                (gate_log_hbm, gate_log_ref),
                (mixw_hbm, mixw_ref),
                (gate_hbm, wg.at[my]),
                (up_hbm, wu.at[my]),
                (down_hbm, wd.at[my]),
            )
        )
    ]
    for copy in own:
        copy.start()

    ids = lax.broadcasted_iota(jnp.int32, (tokens, ep), 1)
    lower = (
        lax.broadcasted_iota(jnp.int32, (tokens, tokens), 1)
        < lax.broadcasted_iota(jnp.int32, (tokens, tokens), 0)
    ).astype(BF16)
    slot_ids = lax.broadcasted_iota(jnp.int32, (tokens, slots), 1)
    taken = jnp.zeros((1, ep), F32)
    routes = routes_ref[...].T
    for side in range(2):
        expert = routes[:, side : side + 1]
        named = (ids == expert).astype(F32)
        before = dot(lower, named.astype(BF16)) + taken
        taken = taken + jnp.sum(named, axis=0, keepdims=True)
        position = jnp.sum(named * before, axis=1, keepdims=True).astype(jnp.int32)
        slot = (expert // per_group) * group_rows + position * per_group + expert % per_group
        picks[side] = jnp.where(slot_ids == slot, 1.0, 0.0).astype(BF16)

    pl.semaphore_wait(barrier, ep - 1 + tp - 1)

    ends = [-(-b // capacity) * LANES for b in PIECES]
    stages = [(gate_hbm, wg, None), (up_hbm, wu, None)] + [
        (down_hbm, wd, pl.ds(a, b - a)) for a, b in zip(ends[:-1], ends[1:])
    ]

    def part_of(i, source, half=None):
        src, dst, cols = stages[i]
        if half is None:
            return (src, dst.at[source]) if cols is None else (
                src.at[:, cols], dst.at[source, :, cols]
            )
        size = dst.shape[1] // 2
        band = pl.ds(half * size, size)
        block = dst.at[source, band] if cols is None else dst.at[source, band, cols]
        return block, block

    def near(i, way):
        src, dst = part_of(i, my)
        peer = (my + (1, 3)[way]) % tp
        return remote(src, dst, wsend.at[i, way], wrecv.at[i, way], at(me, peer))

    def far(i, way):
        src, dst = part_of(i, (my + (3, 1)[way]) % tp, way)
        peer = (my + (1, 3)[way]) % tp
        return remote(src, dst, wsend.at[i, 2 + way], wrecv.at[i, 2 + way], at(me, peer))

    def start_near(i):
        for way in (0, 1):
            near(i, way).start()

    def relay(i):
        for way in (0, 1):
            near(i, way).wait_recv()
            far(i, way).start()

    start_near(0)
    start_near(1)

    def kv_slot(z, x, c):
        return (z * columns + x) * 2 + c

    def z_copy(k):
        return remote(
            kv_hbm,
            kvb.at[me],
            kzsend.at[k],
            kzrecv.at[k],
            at(kv_slot((my_z + k) % planes, my_x, my_c)),
        )

    for k in range(1, planes):

        @pl.when(my_z + k < planes)
        def _(k=k):
            z_copy(k).start()

    own[0].wait()
    normed = rms_scale(x_ref[...].astype(F32), moe_gain_ref[...]).astype(BF16)
    both = picks[0] + picks[1]

    def lay_out(g, value, first):
        for j in range(value.shape[1] // LANES):
            for r in range(capacity):
                wide[g, pl.ds((first + j) * capacity + r, per_group, stride=chunk), :] = value[
                    r * per_group : (r + 1) * per_group, j * LANES : (j + 1) * LANES
                ]

    def gather_up(g, first, last):
        rows = pl.multiple_of(g * group_rows, 16)
        for j in range(first, last):
            for r in range(capacity):
                xs[pl.ds(rows + r * per_group, per_group), j * LANES : (j + 1) * LANES] = wide[
                    g, pl.ds(j * capacity + r, per_group, stride=chunk), :
                ].astype(BF16)

    for pair in range(tiles // 2):
        moved = lax.dot_general(
            both,
            normed[:, pair * 2 * LANES : (pair + 1) * 2 * LANES],
            (((0,), (0,)), ((), ())),
            preferred_element_type=F32,
        )
        for g in range(GROUPS):
            lay_out(g, moved[g * group_rows : (g + 1) * group_rows], 2 * pair)
    for g in range(GROUPS):
        send[g * per_group * chunk : (g + 1) * per_group * chunk, :] = wide[g].astype(BF16)

    def rows_of(e, start=0, size=chunk):
        return pl.ds(pl.multiple_of(e * chunk + start, 16), size)

    def start_dispatch(k, carry):
        e = (me + k) % ep
        remote(
            send.at[rows_of(e)], recv.at[rows_of(me)], dsend, drecv.at[my_group], at(e)
        ).start()
        return carry

    lax.fori_loop(1, ep, start_dispatch, 0)
    recv[rows_of(me), :] = send[rows_of(me), :]

    def amount(rows, sem):
        return pltpu.make_async_copy(send.at[pl.ds(0, rows)], recv.at[pl.ds(0, rows)], sem)

    for i in (1, 2, 3):
        own[i].wait()
    for h in range(heads):
        part = q_ref[:, h * HEAD : (h + 1) * HEAD].astype(F32) * HEAD ** (-0.5)
        qs[h * queries : (h + 1) * queries, :] = jnp.concatenate(
            [part, jnp.zeros_like(part)], axis=1
        ).astype(BF16)
        m_ref[h] = jnp.full((queries, LANES), NEGATIVE, F32)
        l_ref[h] = jnp.zeros((queries, LANES), F32)
        acc_ref[h] = jnp.zeros((queries, LANES), F32)

    def x_copy(k, j):
        slab = kvb.at[kv_slot((my_z + planes - j) % planes, my_x, my_c)]
        return remote(
            slab,
            slab,
            kxsend.at[k * planes + j],
            kxrecv.at[k * planes + j],
            at(kv_slot(my_z, (my_x + k) % columns, my_c)),
        )

    def c_copy(k, j):
        slab = kvb.at[kv_slot((my_z + planes - j) % planes, (my_x + columns - k) % columns, my_c)]
        return remote(
            slab, slab, kcsend.at[k * planes + j], kcrecv.at[k * planes + j], at(me + 1 - 2 * my_c)
        )

    base = gate_log_ref[:, pl.ds(pl.multiple_of(me * queries, LANES), LANES)][:, 0:1]
    slabs = KEY_BLOCK // queries

    def attend(i, masked):
        keys = kvb[pl.ds(i * slabs, slabs)].reshape(KEY_BLOCK, 2 * HEAD)
        start = pl.multiple_of(i * KEY_BLOCK, KEY_BLOCK)
        bias = base - gate_log_ref[:, pl.ds(start, KEY_BLOCK)]
        scores = lax.dot_general(
            qs[...], keys, (((1,), (1,)), ((), ())), preferred_element_type=F32
        )
        weights = []
        factors = []
        for h in range(heads):
            part = scores[h * queries : (h + 1) * queries] + bias[h : h + 1, :]
            if masked:
                key_pos = start + lax.broadcasted_iota(jnp.int32, part.shape, 1)
                query_pos = me * queries + lax.broadcasted_iota(jnp.int32, part.shape, 0)
                part = jnp.where(key_pos <= query_pos, part, NEGATIVE)
            old = m_ref[h]
            new = jnp.maximum(old, jnp.max(part, axis=1, keepdims=True))
            factor = jnp.exp(old - new)
            weight = jnp.exp(part - jnp.concatenate([new] * (KEY_BLOCK // LANES), axis=1))
            summed = weight[:, :LANES]
            for t in range(1, KEY_BLOCK // LANES):
                summed = summed + weight[:, t * LANES : (t + 1) * LANES]
            m_ref[h] = new
            l_ref[h] = l_ref[h] * factor + summed
            weights.append(weight.astype(BF16))
            factors.append(factor)
        moved = dot(jnp.concatenate(weights, axis=0), keys)
        for h in range(heads):
            acc_ref[h] = acc_ref[h] * factors[h] + moved[h * queries : (h + 1) * queries]

    def attend_step(t, carry):
        @pl.when(t <= my_z)
        def _():
            @pl.when(t > 0)
            def _():
                z_copy(t).wait_recv()

            for k in range(1, columns):
                x_copy(k, t).start()
            c_copy(0, t).start()

        @pl.when((t >= 1) & (t <= my_z + 1))
        def _():
            for k in range(1, columns):
                x_copy(k, t - 1).wait_recv()
                c_copy(k, t - 1).start()

        @pl.when(t == planes // 2 + 1)
        def _():
            relay(0)
            start_near(2)

        @pl.when(t >= 2)
        def _():
            for k in range(columns):
                c_copy(k, t - 2).wait_recv()
            first = (my_z + 2 - t) * columns

            def whole(i, carry):
                attend(i, False)
                return carry

            lax.fori_loop(first, first + jnp.where(t == 2, my_x, columns), whole, 0)

            @pl.when(t == 2)
            def _():
                attend(me // slabs, True)

        return carry

    lax.fori_loop(0, my_z + 3, attend_step, 0)

    @pl.when(my_z + 2 < planes // 2 + 1)
    def _():
        relay(0)
        start_near(2)

    relay(1)

    own[4].wait()
    attended = jnp.concatenate(
        [acc_ref[h][:, HEAD:] / jnp.sum(l_ref[h], axis=1, keepdims=True) for h in range(heads)],
        axis=1,
    ).astype(BF16)
    mixb[...] = dot(attended, mixw_ref[...]).astype(BF16)
    share = queries // tp

    def mix_copy(k):
        t = (my + k) % tp
        return remote(
            mixb.at[pl.ds(pl.multiple_of(t * share, 16), share)],
            mixr.at[k],
            msend.at[k],
            mrecv.at[k],
            at(me, t),
        )

    mixr[0] = mixb[pl.ds(pl.multiple_of(my * share, 16), share), :]

    for i in (5, 6, 7):
        own[i].wait()
    for g in range(GROUPS):

        @pl.when(g == my_group)
        def _(g=g):
            amount((per_group - 1) * chunk, drecv.at[g]).wait()

        @pl.when(g != my_group)
        def _(g=g):
            amount(per_group * chunk, drecv.at[g]).wait()

    def spread(g, carry):
        size = per_group * chunk
        wide[g] = recv[pl.ds(pl.multiple_of(g * size, 16), size), :].astype(F32)
        gather_up(g, 0, tiles)
        return carry

    lax.fori_loop(0, GROUPS, spread, 0)

    def expand(k, carry):
        q = (my + k) % tp
        up_part = dot(xs[...], wu[q])
        gate_part = dot(xs[...], wg[q])
        hid[q] = (gate_part / (1.0 + jnp.exp(-gate_part)) * up_part).astype(BF16)
        return carry

    def expand_step(i, carry):
        @pl.when(i == 3)
        def _():
            relay(2)
            for m in range(3, min(5, len(stages))):
                start_near(m)
            for m in (0, 1):
                for way in (0, 1):
                    far(m, way).wait_recv()

        return expand(i + (i // 2) * (5 - 2 * i), carry)

    lax.fori_loop(0, tp, expand_step, 0)

    pieces = list(zip(PIECES[:-1], PIECES[1:]))

    def contract(p, i):
        low, high = pieces[p]
        g = (i + my_group) % GROUPS
        rows = pl.ds(pl.multiple_of(g * group_rows, 16), group_rows)
        first, last = ends[p], ends[p + 1]
        total = jnp.zeros((group_rows, last - first), F32)
        for q in range(tp):
            total = total + dot(hid[q, rows, :], wd[q, :, first:last])
        lay_out(g, total, first // LANES)
        for s in range(per_group):
            outb[rows_of(g * per_group + s, low, high - low), :] = wide[
                g, s * chunk + low : s * chunk + high, :
            ].astype(BF16)

        def start_combine(j, carry):
            s = g * per_group + (j + me) % per_group

            @pl.when(s != me)
            def _():
                remote(
                    outb.at[rows_of(s, low, high - low)],
                    ret.at[rows_of(me, low, high - low)],
                    csend,
                    crecv.at[p],
                    at(s),
                ).start()

            return carry

        lax.fori_loop(0, per_group, start_combine, 0)

    for p in range(len(pieces)):
        if p > 0:
            relay(2 + p)
            if p + 2 < len(pieces):
                start_near(4 + p)
        if p == len(pieces) - 1:
            for k in range(1, tp):
                mix_copy(k).start()
        for way in (0, 1):
            far(2 + p, way).wait_recv()

        def contract_step(i, carry, p=p):
            contract(p, i)
            return carry

        lax.fori_loop(0, GROUPS, contract_step, 0)
    ret[rows_of(me), :] = outb[rows_of(me), :]

    weights = weight_ref[...].T
    for p, (low, high) in enumerate(pieces):
        amount((ep - 1) * (high - low), crecv.at[p]).wait()
        first, last = low // capacity, high // capacity

        def take_in(g, carry, low=low, high=high, first=first, last=last):
            for s in range(per_group):
                wide[g, s * chunk + low : s * chunk + high, :] = ret[
                    rows_of(g * per_group + s, low, high - low), :
                ].astype(F32)
            gather_up(g, first, last)
            return carry

        lax.fori_loop(0, GROUPS, take_in, 0)
        cols = slice(first * LANES, last * LANES)
        chosen = xs[:, cols]
        total = weights[:, 0:1] * dot(picks[0], chosen)
        total = total + weights[:, 1:2] * dot(picks[1], chosen)
        moe_out[:, cols] = total.astype(BF16)
        if p == len(pieces) - 2:
            for k in range(1, tp):
                mix_copy(k).wait()
            summed = mixr[0].astype(F32)
            for part in range(1, tp):
                summed = summed + mixr[part].astype(F32)
            mix_out[...] = rms_scale(summed, mix_gain_ref[...]).astype(BF16)

    amount((ep - 1) * chunk, dsend).wait()
    amount((ep - 1) * chunk, csend).wait()
    for k in range(1, planes):

        @pl.when(my_z + k < planes)
        def _(k=k):
            z_copy(k).wait_send()

    def wait_kv(j, carry):
        c_copy(0, j).wait_send()
        for k in range(1, columns):
            x_copy(k, j).wait_send()
            c_copy(k, j).wait_send()
        return carry

    lax.fori_loop(0, my_z + 1, wait_kv, 0)
    for i in range(len(stages)):
        for way in (0, 1):
            near(i, way).wait_send()
            far(i, way).wait_send()


def body(
    planes,
    columns,
    queries,
    keys_values,
    log_gate_cum,
    mix_weight,
    mix_gain,
    moe_in,
    moe_gain,
    routes,
    route_weight,
    expert_gate,
    expert_up,
    expert_down,
):
    ep = planes * columns * 2
    tp = 4
    tokens, model = moe_in.shape
    tiles = model // LANES
    capacity = 3 * routes.shape[1] * tokens // (2 * ep)
    slots = ep * capacity
    rows = queries.shape[0]
    heads = queries.shape[1] // HEAD
    depth, width = expert_gate.shape[1:]
    stages = 1 + len(PIECES)
    vmem = pl.BlockSpec(memory_space=pltpu.VMEM)
    hbm = pl.BlockSpec(memory_space=pl.ANY)
    dma = pltpu.SemaphoreType.DMA
    return pl.pallas_call(
        functools.partial(step_kernel, planes, columns),
        out_shape=(
            jax.ShapeDtypeStruct((rows // tp, model), BF16),
            jax.ShapeDtypeStruct((tokens, model), BF16),
        ),
        in_specs=[hbm] * 4 + [vmem, hbm, vmem, vmem, vmem] + [hbm] * 3,
        out_specs=(vmem, vmem),
        scratch_shapes=[
            pltpu.VMEM((tokens, model), BF16),
            pltpu.VMEM(queries.shape, BF16),
            pltpu.VMEM(log_gate_cum.shape, F32),
            pltpu.VMEM(mix_weight.shape, BF16),
            pltpu.VMEM((tp, depth, width), BF16),
            pltpu.VMEM((tp, depth, width), BF16),
            pltpu.VMEM((tp, width, model), BF16),
            pltpu.VMEM((ep, rows, 2 * HEAD), BF16),
            pltpu.VMEM((2, tokens, slots), BF16),
            pltpu.VMEM((slots * tiles, LANES), BF16),
            pltpu.VMEM((slots * tiles, LANES), BF16),
            pltpu.VMEM((slots, model), BF16),
            pltpu.VMEM((tp, slots, width), BF16),
            pltpu.VMEM((GROUPS, slots * tiles // GROUPS, LANES), F32),
            pltpu.VMEM((slots * tiles, LANES), BF16),
            pltpu.VMEM((slots * tiles, LANES), BF16),
            pltpu.VMEM((heads * rows, 2 * HEAD), BF16),
            pltpu.VMEM((heads, rows, LANES), F32),
            pltpu.VMEM((heads, rows, LANES), F32),
            pltpu.VMEM((heads, rows, LANES), F32),
            pltpu.VMEM((rows, model), BF16),
            pltpu.VMEM((tp, rows // tp, model), BF16),
            dma((8,)),
            dma((stages, tp)),
            dma((stages, tp)),
            dma((planes,)),
            dma((planes,)),
            dma((columns * planes,)),
            dma((columns * planes,)),
            dma((columns * planes,)),
            dma((columns * planes,)),
            dma,
            dma((GROUPS,)),
            dma,
            dma((len(PIECES) - 1,)),
            dma((tp,)),
            dma((tp,)),
        ],
        compiler_params=pltpu.CompilerParams(
            collective_id=0, has_side_effects=True, vmem_limit_bytes=64000 * 1024
        ),
        name="layer_step",
    )(
        queries,
        keys_values,
        log_gate_cum,
        mix_weight,
        mix_gain[None],
        moe_in,
        moe_gain[None],
        routes.T,
        route_weight.T,
        expert_gate[0],
        expert_up[0],
        expert_down[0],
    )


def solution(mesh, planes=8, columns=4):
    in_specs = (
        P("ep", "tp"),
        P("ep", "tp"),
        P("tp", None),
        P("tp", None),
        P(),
        P(("ep", "tp"), None),
        P(),
        P(("ep", "tp"), None),
        P(("ep", "tp"), None),
        P("ep", None, "tp"),
        P("ep", None, "tp"),
        P("ep", "tp", None),
    )
    out_specs = (P(("ep", "tp"), None), P(("ep", "tp"), None))
    return jax.shard_map(
        functools.partial(body, planes, columns),
        mesh=mesh,
        in_specs=in_specs,
        out_specs=out_specs,
        check_vma=False,
    )
```

time: 194 us -> 159 us (0.82)
  Pallas kernels: 186 us -> 155 us
  local copies, waits for them, and re-layouts: 7.03 us -> 3.76 us
    pallas_call x3 -> x1, Pallas kernels: 186 us -> 155 us  [body(): pl.pallas_call(functools.partial(step_kernel, planes, columns), out_shape...]
    unnamed x20 -> x2, local copies, waits for them, and re-layouts: 7.03 us -> 3.76 us
where the time goes in v2:
time: 159 us
  Pallas kernels  155 us (97%)
  local copies, waits for them, and re-layouts  3.76 us (2%)
    pallas_call x1, Pallas kernels, body(): pl.pallas_call(functools.partial(step_kernel, planes, columns), out_shape...  155 us
    unnamed x2, local copies, waits for them, and re-layouts  3.76 us

profile of v2, /device:TPU:1, one launch (start us, length us, event | category | flops | bytes accessed | tf_op | source)
XLA Modules:
  0.0 159.0 jit_solution(5874777497535284211)
XLA Ops:
  0.6 154.6 %layer_step.1 = (bf16[64,2048]{1,0:T(8,128)(2,1)}, bf16[192,2048]{1,0:T(8,128)(2,1)}) custom-call(bf16[256,256]{1,0:T(8,128)(2,1)} %q_hbm.1, bf16[256,128]{1,0:T(8,128)(2,1)} %kv_hbm.1, f32[4,16384]{1,0:T(4,128)} %gate_log_hbm.1, bf16[256,2048]{1,0:T(8,128)(2,1)} %mixw_hbm.1, f32[1,2048]{1,0:T(1,128)} %bitcast.10, bf16[192,2048]{1,0:T(8,128)(2,1)} %x_hbm.1, ...), custom_call_target="tpu_custom_call" | custom-call | tf_op jit(solution)/shard_map/layer_step/pallas_call | solution.py:565
  155.3 1.7 %copy.16 = bf16[64,2048]{1,0:T(8,128)(2,1)} copy(bf16[64,2048]{1,0:T(8,128)(2,1)} %get-tuple-element.4) | data formatting | bytes 524288
  157.0 2.1 %copy.17 = bf16[192,2048]{1,0:T(8,128)(2,1)} copy(bf16[192,2048]{1,0:T(8,128)(2,1)} %get-tuple-element.5) | data formatting | bytes 1572864

commit v3 on v2

--- a/solution.py
+++ b/solution.py
@@ -13,7 +13,8 @@
 LANES = 128
 KEY_BLOCK = 512
 GROUPS = 4
-PIECES = (0, 32, 64, 96, 144)
+STORES = 3
+PIECES = (0, 32, 64, 96, 128, 144)
 MESH = pl.DeviceIdType.MESH
 F32 = jnp.float32
 BF16 = jnp.bfloat16
@@ -251,7 +252,7 @@
         return pl.ds(pl.multiple_of(e * chunk + start, 16), size)
 
     def start_dispatch(k, carry):
-        e = (me + k) % ep
+        e = (me + 1 + (k + ep // 3) % (ep - 1)) % ep
         remote(
             send.at[rows_of(e)], recv.at[rows_of(me)], dsend, drecv.at[my_group], at(e)
         ).start()
@@ -437,7 +438,7 @@
 
     def contract(p, i):
         low, high = pieces[p]
-        g = (i + my_group) % GROUPS
+        g = (i + my_group + GROUPS // 2) % GROUPS
         rows = pl.ds(pl.multiple_of(g * group_rows, 16), group_rows)
         first, last = ends[p], ends[p + 1]
         total = jnp.zeros((group_rows, last - first), F32)
@@ -531,6 +532,26 @@
         for way in (0, 1):
             near(i, way).wait_send()
             far(i, way).wait_send()
+
+
+def store_kernel(mixed_in, experts_in, mixed_out, experts_out, mixed, experts, load_sem, save_sem):
+    band = experts.shape[0] // STORES
+    bands = [pl.ds(i * band, band) for i in range(STORES)]
+    views = [(experts_in.at[b], experts.at[b], experts_out.at[b]) for b in bands]
+    views.append((mixed_in, mixed, mixed_out))
+    loads = [
+        pltpu.make_async_copy(src, mid, load_sem.at[i]) for i, (src, mid, _) in enumerate(views)
+    ]
+    saves = [
+        pltpu.make_async_copy(mid, dst, save_sem.at[i]) for i, (_, mid, dst) in enumerate(views)
+    ]
+    for load in loads:
+        load.start()
+    for load, save in zip(loads, saves):
+        load.wait()
+        save.start()
+    for save in saves:
+        save.wait()
 
 
 def body(
@@ -562,7 +583,7 @@
     vmem = pl.BlockSpec(memory_space=pltpu.VMEM)
     hbm = pl.BlockSpec(memory_space=pl.ANY)
     dma = pltpu.SemaphoreType.DMA
-    return pl.pallas_call(
+    mixed, experts = pl.pallas_call(
         functools.partial(step_kernel, planes, columns),
         out_shape=(
             jax.ShapeDtypeStruct((rows // tp, model), BF16),
@@ -628,6 +649,25 @@
         expert_down[0],
     )
 
+    outs = (
+        jax.ShapeDtypeStruct(mixed.shape, BF16),
+        jax.ShapeDtypeStruct(experts.shape, BF16),
+    )
+    return pl.pallas_call(
+        store_kernel,
+        out_shape=outs,
+        in_specs=[hbm, hbm],
+        out_specs=(hbm, hbm),
+        scratch_shapes=[
+            pltpu.VMEM(mixed.shape, BF16),
+            pltpu.VMEM(experts.shape, BF16),
+            dma((1 + STORES,)),
+            dma((1 + STORES,)),
+        ],
+        compiler_params=pltpu.CompilerParams(vmem_limit_bytes=64000 * 1024),
+        name="store",
+    )(mixed, experts)
+
 
 def solution(mesh, planes=8, columns=4):
     in_specs = (

time: 159 us -> 153 us (0.962)
  local copies, waits for them, and re-layouts: 3.76 us -> 0 us
  Pallas kernels: 155 us -> 152 us
    pallas_call x1, Pallas kernels: 155 us -> 150 us  [body(): pl.pallas_call(functools.partial(step_kernel, planes, columns), out_shape...]
    unnamed x2 -> x0, local copies, waits for them, and re-layouts: 3.76 us -> none
    pallas_call x0 -> x1, Pallas kernels: none -> 1.98 us  [body(): pl.pallas_call(store_kernel, out_shape=outs, in_specs=[hbm, hbm], out_spe...]
where the time goes in v3:
time: 153 us
  Pallas kernels  152 us (99%)
    pallas_call x1, Pallas kernels, body(): pl.pallas_call(functools.partial(step_kernel, planes, columns), out_shape...  150 us

profile of v3, /device:TPU:1, one launch (start us, length us, event | category | flops | bytes accessed | tf_op | source)
XLA Modules:
  0.0 153.1 jit_solution(3905931922049603187)
XLA Ops:
  0.6 150.5 %layer_step.1 = (bf16[64,2048]{1,0:T(8,128)(2,1)}, bf16[192,2048]{1,0:T(8,128)(2,1)}) custom-call(bf16[256,256]{1,0:T(8,128)(2,1)} %q_hbm.1, bf16[256,128]{1,0:T(8,128)(2,1)} %kv_hbm.1, f32[4,16384]{1,0:T(4,128)} %gate_log_hbm.1, bf16[256,2048]{1,0:T(8,128)(2,1)} %mixw_hbm.1, f32[1,2048]{1,0:T(1,128)} %bitcast.10, bf16[192,2048]{1,0:T(8,128)(2,1)} %x_hbm.1, ...), custom_call_target="tpu_custom_call" | custom-call | tf_op jit(solution)/shard_map/layer_step/pallas_call | solution.py:586
  151.1 2.0 %store.1 = (bf16[64,2048]{1,0:T(8,128)(2,1)}, bf16[192,2048]{1,0:T(8,128)(2,1)}) custom-call(bf16[64,2048]{1,0:T(8,128)(2,1)} %get-tuple-element.4.mixed_in, bf16[192,2048]{1,0:T(8,128)(2,1)} %get-tuple-element.5.experts_in), custom_call_target="tpu_custom_call" | custom-call | tf_op jit(solution)/shard_map/store/pallas_call | solution.py:656
